TPU v7x, 256 devices: a 4x2x16 block of a 4x16x16 slice. The times are simulated.
256 devices in a mesh: grp: 2 (over y), fs: 32 (over z, core), tp: 4 (over x).
Axes of the slice: x: 4, y: 2, z: 16, core: 2. Of those that a mesh axis runs over, the one named last changes fastest.
The devices are a block of a 4x16x16 slice.
Arguments:
- prompt: bfloat16 [8, 1024, 2048], P(('grp', 'tp')), parts along dimension 0, may hold values from -6 to 6
- gate_first: float32 [2048, 5632], P('fs', 'tp'), may hold values from -0.125 to 0.125
- up_first: float32 [2048, 5632], P('fs', 'tp'), may hold values from -0.125 to 0.125
- down_first: float32 [5632, 2048], P('fs', 'tp'), may hold values from -0.3125 to 0.3125
- norm_gain: float32 [2048], replicated, may hold values from 0.1 to 1.9
- gate_second: float32 [2048, 5632], P('fs', 'tp'), may hold values from -0.125 to 0.125
- up_second: float32 [2048, 5632], P('fs', 'tp'), may hold values from -0.125 to 0.125
- down_second: float32 [5632, 2048], P('fs', 'tp'), may hold values from -0.3125 to 0.3125
Outputs:
- result: bfloat16 [8, 1024, 2048], P(('grp', 'tp'), 'fs'), parts along dimension 0
- gate_one: bfloat16 [4096, 5632], P('grp', 'fs'), parts along dimension 0
- up_one: bfloat16 [4096, 5632], P('grp', 'fs'), parts along dimension 0
- down_one: bfloat16 [5632, 4096], P('fs', 'grp'), parts along dimension 1
- gate_two: bfloat16 [4096, 5632], P('grp', 'fs'), parts along dimension 0
- up_two: bfloat16 [4096, 5632], P('grp', 'fs'), parts along dimension 0
- down_two: bfloat16 [5632, 4096], P('fs', 'grp'), parts along dimension 1
There are 2 independent parts, one for each index of `grp`. A program takes and returns all parts, laid end to end along the dimension named above; an argument that names none is the same for every part. Nothing has to cross between parts.
All inputs are finite; a program needn't handle non-finite values.
Results may differ from a plain program's by a relative error of at most 0.029.
Values may be sent and summed in bfloat16 or wider, within the bound.
A program may use at most 64 MiB of HBM per device.

v0:
```python
import jax
import jax.numpy as jnp
from jax import lax
from jax.sharding import Mesh
from jax.sharding import PartitionSpec as P

FS = ("fs_0", "fs_1")


norm_eps = 1e-05
deep_alpha = 2.0**0.25
half_step = 0.5


def reduced_to_own(pieces, axes, sequence):
    inside = pieces.shape[1:]
    pieces = pieces.reshape(*(lax.axis_size(a) for a in axes), *inside)
    pieces = jnp.moveaxis(pieces, sequence, range(len(axes))).reshape(-1, *inside)
    for k in sequence:
        pieces = lax.psum_scatter(pieces, axes[k], scatter_dimension=0, tiled=True)
    return pieces[0]


def cut_along(value, dim, size):
    before, after = (value.shape[:dim], value.shape[dim + 1 :])
    return jnp.moveaxis(value.reshape(*before, size, -1, *after), dim, 0)


def scatter_axes(value, axes, sequence, dim):
    size = lax.axis_size(axes)
    return reduced_to_own(cut_along(value, dim, size), axes, sequence)


def plain_norm(values):
    row_mean = jnp.mean(values, axis=-1, keepdims=True)
    centred = values - row_mean
    variance = jnp.mean(centred * centred, axis=-1, keepdims=True)
    return centred * lax.rsqrt(variance + norm_eps)


def gated_hidden(inputs, gate_proj, up_proj):
    gate_act = jnp.dot(inputs, gate_proj, preferred_element_type=jnp.float32)
    up_act = jnp.dot(inputs, up_proj, preferred_element_type=jnp.float32)
    return (jax.nn.silu(gate_act) * up_act).astype(jnp.bfloat16)


def relay_weights(gate_proj, up_proj, down_proj):
    gate_rows, up_rows, down_mine = (
        lax.all_gather(gate_proj, "tp", axis=1, tiled=True),
        lax.all_gather(up_proj, "tp", axis=1, tiled=True),
        lax.all_gather(down_proj, "tp", axis=1, tiled=True),
    )
    gate_mine, up_mine = (
        lax.all_to_all(gate_rows, FS, split_axis=1, concat_axis=0, tiled=True),
        lax.all_to_all(up_rows, FS, split_axis=1, concat_axis=0, tiled=True),
    )
    return (gate_mine, up_mine, down_mine)


def row_terms(hidden, down_proj):
    return jnp.dot(hidden, down_proj, preferred_element_type=jnp.float32)


def body(prompt, gate_first, up_first, down_first, norm_gain, gate_second, up_second, down_second):
    fs_index = lax.axis_index(FS)
    row_block = gate_first.shape[0]
    gain_rows = lax.dynamic_slice_in_dim(norm_gain, fs_index * row_block, row_block, 0)
    gate_one, up_one, down_one = relay_weights(
        gate_first.astype(jnp.bfloat16),
        up_first.astype(jnp.bfloat16),
        down_first.astype(jnp.bfloat16),
    )
    gate_two, up_two, down_two = relay_weights(
        (gain_rows[:, None] * gate_second).astype(jnp.bfloat16),
        (gain_rows[:, None] * up_second).astype(jnp.bfloat16),
        down_second.astype(jnp.bfloat16),
    )
    tokens = prompt.reshape(-1, prompt.shape[-1])
    own_count = tokens.shape[0] // lax.axis_size(FS)
    own_first = fs_index * own_count
    hidden_one = gated_hidden(tokens, gate_one, up_one)
    own_tokens = lax.dynamic_slice_in_dim(tokens, own_first, own_count, 0)
    ffn_one = scatter_axes(
        row_terms(hidden_one, down_one).astype(jnp.bfloat16), FS, (1, 0), 0
    ).astype(jnp.float32)
    normed_own = plain_norm(
        deep_alpha * own_tokens.astype(jnp.float32) + half_step * ffn_one
    ).astype(jnp.bfloat16)
    hidden_two = gated_hidden(lax.all_gather(normed_own, FS, axis=0, tiled=True), gate_two, up_two)
    ffn_two = scatter_axes(
        row_terms(hidden_two, down_two).astype(jnp.bfloat16), FS, (1, 0), 0
    ).astype(jnp.float32)
    residual_two = deep_alpha * norm_gain * normed_own.astype(jnp.float32)
    result = plain_norm(residual_two + half_step * ffn_two).astype(jnp.bfloat16)
    return (
        result.reshape(1, result.shape[0], result.shape[-1]),
        gate_one,
        up_one,
        down_one,
        gate_two,
        up_two,
        down_two,
    )


def solution(mesh):
    torus = Mesh(
        mesh.devices.reshape(mesh.shape["grp"], 16, 2, mesh.shape["tp"]),
        ("grp", "fs_0", "fs_1", "tp"),
    )
    placed = (
        P(("grp", "tp"), None, None),
        P(FS, "tp"),
        P(FS, "tp"),
        P(FS, "tp"),
        P(),
        P(FS, "tp"),
        P(FS, "tp"),
        P(FS, "tp"),
    )
    return jax.shard_map(
        body,
        mesh=torus,
        in_specs=placed,
        out_specs=(
            P(("grp", "tp"), FS, None),
            P("grp", FS),
            P("grp", FS),
            P(FS, "grp"),
            P("grp", FS),
            P("grp", FS),
            P(FS, "grp"),
        ),
        check_vma=False,
    )
```

profile of v0, /device:TPU:34, one launch (start us, length us, event | category | flops | bytes accessed | tf_op | source)
XLA Modules:
  0.0 540.0 jit_solution(11706451847986128299)
XLA Ops:
  8.2 29.5 %all_gather.21 = bf16[64,5632]{1,0:T(8,128)(2,1)S(1)} all-gather(bf16[64,1408]{1,0:T(8,128)(2,1)S(1)} %convert_element_type.62), channel_id=1, replica_groups=mesh['grp'=2,'fs_0'=16,'fs_1'=2,'tp'=4] {'tp'}, dimensions={1}, use_global_device_ids=true | all-gather | bytes 901120 | tf_op jit(solution)/shard_map/all_gather | solution.py:49
  37.8 2.0 all_to_all.56
  41.4 9.7 %all-to-all-start = ((bf16[64,32,176]{2,0,1:T(8,128)(2,1)}), bf16[64,32,176]{2,0,1:T(8,128)(2,1)S(1)}, u32[]{:S(2)}, u32[]{:S(2)}) async-start(bf16[64,32,176]{2,0,1:T(8,128)(2,1)} %copy.21), calls=%async_computation | async-start | bytes 2097152 | tf_op jit(solution)/shard_map/all_to_all | solution.py:54
  51.2 14.4 %all_gather.22 = bf16[64,5632]{1,0:T(8,128)(2,1)S(1)} all-gather(bf16[64,1408]{1,0:T(8,128)(2,1)S(1)} %convert_element_type.63), channel_id=1, replica_groups=mesh['grp'=2,'fs_0'=16,'fs_1'=2,'tp'=4] {'tp'}, dimensions={1}, use_global_device_ids=true | all-gather | bytes 901120 | tf_op jit(solution)/shard_map/all_gather | solution.py:50
  65.5 2.0 all_to_all.60
  69.1 37.3 %all-to-all-done = bf16[64,32,176]{2,0,1:T(8,128)(2,1)S(1)} async-done(((bf16[64,32,176]{2,0,1:T(8,128)(2,1)}), bf16[64,32,176]{2,0,1:T(8,128)(2,1)S(1)}, u32[]{:S(2)}, u32[]{:S(2)}) %all-to-all-start) | async-done | bytes 720928 | tf_op jit(solution)/shard_map/all_to_all | solution.py:54
  106.4 4.8 all-to-all-start.1
  111.4 14.2 %all_gather.23 = bf16[176,2048]{1,0:T(8,128)(2,1)S(1)} all-gather(bf16[176,512]{1,0:T(8,128)(2,1)S(1)} %convert_element_type.65), channel_id=1, replica_groups=mesh['grp'=2,'fs_0'=16,'fs_1'=2,'tp'=4] {'tp'}, dimensions={1}, use_global_device_ids=true | all-gather | bytes 901120 | tf_op jit(solution)/shard_map/all_gather | solution.py:51
  125.6 4.0 fusion.2
  129.6 37.3 %all-to-all-done.1 = bf16[64,32,176]{2,0,1:T(8,128)(2,1)S(1)} async-done(((bf16[64,32,176]{2,0,1:T(8,128)(2,1)}), bf16[64,32,176]{2,0,1:T(8,128)(2,1)S(1)}, u32[]{:S(2)}, u32[]{:S(2)}) %all-to-all-start.1) | async-done | bytes 720928 | tf_op jit(solution)/shard_map/all_to_all | solution.py:55
  167.0 7.0 %convolution_convert_fusion.1 = bf16[1024,2048]{1,0:T(8,128)(2,1)} fusion(bf16[176,2048]{1,0:T(8,128)(2,1)S(1)} %all_gather.23, bf16[2048,176]{1,0:T(8,128)(2,1)S(1)} %bitcast.57, bf16[1,1024,2048]{2,1,0:T(8,128)(2,1)} %param.8, f32[1024,176]{0,1:T(8,128)S(1)} %fusion.2), kind=kOutput, calls=%fused_computation.5 | convolution fusion | flops 1479573504 | bytes 10551296 | tf_op jit(solution)/shard_map/dot_general | solution.py:61
  173.9 4.7 copy.23
  178.8 12.5 %reduce-scatter.5.cloned.1.call-done = bf16[16,32,2048]{2,1,0:T(8,128)(2,1)} async-done(((bf16[32,32,2048]{2,1,0:T(8,128)(2,1)}), bf16[16,32,2048]{2,1,0:T(8,128)(2,1)}) %reduce-scatter.5.cloned.1.call-update) | async-done | bytes 2097168 | tf_op jit(solution)/shard_map/reduce_scatter | solution.py:20
  191.4 75.9 %reduce-scatter.7.cloned.1.call-done = bf16[1,32,2048]{2,1,0:T(8,128)(2,1)} async-done(((bf16[16,32,2048]{2,1,0:T(8,128)(2,1)}), bf16[1,32,2048]{2,1,0:T(8,128)(2,1)}) %reduce-scatter.7.cloned.1.call-update) | async-done | bytes 131088 | tf_op jit(solution)/shard_map/reduce_scatter | solution.py:20
  269.7 1.7 multiply_convert_fusion.3
  271.7 14.1 %all_gather.25 = bf16[64,5632]{1,0:T(8,128)(2,1)} all-gather(bf16[64,1408]{1,0:T(8,128)(2,1)S(1)} %get-tuple-element.14), channel_id=1, replica_groups=mesh['grp'=2,'fs_0'=16,'fs_1'=2,'tp'=4] {'tp'}, dimensions={1}, use_global_device_ids=true | all-gather | bytes 901120 | tf_op jit(solution)/shard_map/all_gather | solution.py:49
  285.8 3.0 all_to_all.64
  290.4 9.7 %all-to-all-start.2 = ((bf16[64,32,176]{2,0,1:T(8,128)(2,1)}), bf16[64,32,176]{2,0,1:T(8,128)(2,1)S(1)}, u32[]{:S(2)}, u32[]{:S(2)}) async-start(bf16[64,32,176]{2,0,1:T(8,128)(2,1)} %copy.24), calls=%async_computation.4 | async-start | bytes 2097152 | tf_op jit(solution)/shard_map/all_to_all | solution.py:54
  300.1 14.3 %all_gather.26 = bf16[64,5632]{1,0:T(8,128)(2,1)} all-gather(bf16[64,1408]{1,0:T(8,128)(2,1)S(1)} %get-tuple-element.15), channel_id=1, replica_groups=mesh['grp'=2,'fs_0'=16,'fs_1'=2,'tp'=4] {'tp'}, dimensions={1}, use_global_device_ids=true | all-gather | bytes 901120 | tf_op jit(solution)/shard_map/all_gather | solution.py:50
  314.4 3.8 all_to_all.68
  318.2 2.8 copy.25
  321.0 44.7 %all-to-all-done.2 = bf16[64,32,176]{2,0,1:T(8,128)(2,1)S(1)} async-done(((bf16[64,32,176]{2,0,1:T(8,128)(2,1)}), bf16[64,32,176]{2,0,1:T(8,128)(2,1)S(1)}, u32[]{:S(2)}, u32[]{:S(2)}) %all-to-all-start.2) | async-done | bytes 720928 | tf_op jit(solution)/shard_map/all_to_all | solution.py:54
  365.7 5.7 %all-to-all-start.3 = ((bf16[64,32,176]{2,0,1:T(8,128)(2,1)}), bf16[64,32,176]{2,0,1:T(8,128)(2,1)}, u32[]{:S(2)}, u32[]{:S(2)}) async-start(bf16[64,32,176]{2,0,1:T(8,128)(2,1)} %copy.25), calls=%async_computation.5 | async-start | bytes 2097152 | tf_op jit(solution)/shard_map/all_to_all | solution.py:55
  371.5 14.5 %all_gather.27 = bf16[176,2048]{1,0:T(8,128)(2,1)} all-gather(bf16[176,512]{1,0:T(8,128)(2,1)S(1)} %convert_element_type.74), channel_id=1, replica_groups=mesh['grp'=2,'fs_0'=16,'fs_1'=2,'tp'=4] {'tp'}, dimensions={1}, use_global_device_ids=true | all-gather | bytes 901120 | tf_op jit(solution)/shard_map/all_gather | solution.py:51
  386.0 4.6 fusion.29
  390.6 36.6 %all-to-all-done.3 = bf16[64,32,176]{2,0,1:T(8,128)(2,1)} async-done(((bf16[64,32,176]{2,0,1:T(8,128)(2,1)}), bf16[64,32,176]{2,0,1:T(8,128)(2,1)}, u32[]{:S(2)}, u32[]{:S(2)}) %all-to-all-start.3) | async-done | bytes 720928 | tf_op jit(solution)/shard_map/all_to_all | solution.py:55
  427.2 7.7 %convolution_convert_fusion = bf16[1024,2048]{1,0:T(8,128)(2,1)} fusion(bf16[176,2048]{1,0:T(8,128)(2,1)} %all_gather.27, bf16[1024,2048]{1,0:T(8,128)(2,1)} %all-gather.2.cloned.1.call-done, bf16[2048,176]{1,0:T(8,128)(2,1)} %bitcast.12, f32[1024,176]{0,1:T(8,128)} %fusion.29), kind=kOutput, calls=%fused_computation.4 | convolution fusion | flops 1479573504 | bytes 10551296 | tf_op jit(solution)/shard_map/dot_general | solution.py:61
  434.9 4.7 copy.26
  439.7 11.8 %reduce-scatter.9.cloned.1.call-done = bf16[16,32,2048]{2,1,0:T(8,128)(2,1)} async-done(((bf16[32,32,2048]{2,1,0:T(8,128)(2,1)}), bf16[16,32,2048]{2,1,0:T(8,128)(2,1)}) %reduce-scatter.9.cloned.1.call-update) | async-done | bytes 2097168 | tf_op jit(solution)/shard_map/reduce_scatter | solution.py:20
  452.9 2.3 copy.30
  457.6 70.1 %reduce-scatter.11.cloned.1.call-done = bf16[1,32,2048]{2,1,0:T(8,128)(2,1)} async-done(((bf16[16,32,2048]{2,1,0:T(8,128)(2,1)}), bf16[1,32,2048]{2,1,0:T(8,128)(2,1)}) %reduce-scatter.11.cloned.1.call-update) | async-done | bytes 131088 | tf_op jit(solution)/shard_map/reduce_scatter | solution.py:20
  529.9 1.9 multiply_convert_fusion.2
  (52 shorter events, 16.6 us)
Async XLA Ops:
  7.2 43.9 %copy-start.3 = (f32[64,1408]{1,0:T(8,128)S(1)}, f32[64,1408]{1,0:T(8,128)}, u32[]{:S(2)}) copy-start(f32[64,1408]{1,0:T(8,128)} %param.10) | copy-start | bytes 1081348
  41.4 65.0 %all-to-all-start = ((bf16[64,32,176]{2,0,1:T(8,128)(2,1)}), bf16[64,32,176]{2,0,1:T(8,128)(2,1)S(1)}, u32[]{:S(2)}, u32[]{:S(2)}) async-start(bf16[64,32,176]{2,0,1:T(8,128)(2,1)} %copy.21), calls=%async_computation | async-start | bytes 2097152 | tf_op jit(solution)/shard_map/all_to_all | solution.py:54
  51.1 60.2 %copy-start.4 = (f32[176,512]{1,0:T(8,128)S(1)}, f32[176,512]{1,0:T(8,128)}, u32[]{:S(2)}) copy-start(f32[176,512]{1,0:T(8,128)} %param.11) | copy-start | bytes 1081348
  106.4 60.6 %all-to-all-start.1 = ((bf16[64,32,176]{2,0,1:T(8,128)(2,1)}), bf16[64,32,176]{2,0,1:T(8,128)(2,1)S(1)}, u32[]{:S(2)}, u32[]{:S(2)}) async-start(bf16[64,32,176]{2,0,1:T(8,128)(2,1)} %copy.22), calls=%async_computation.1 | async-start | bytes 2097152 | tf_op jit(solution)/shard_map/all_to_all | solution.py:55
  111.3 80.0 %reduce-scatter.5.cloned.1.call-start = ((), (), s32[]{:S(2)}) async-start(), calls=%async_computation.8 | async-start | bytes 6291456 | tf_op jit(solution)/shard_map/reduce_scatter | solution.py:20
  125.6 41.4 %copy-start = (bf16[176,2048]{1,0:T(8,128)(2,1)}, bf16[176,2048]{1,0:T(8,128)(2,1)S(1)}, u32[]{:S(2)}) copy-start(bf16[176,2048]{1,0:T(8,128)(2,1)S(1)} %all_gather.23) | copy-start | bytes 2162692
  178.7 92.8 %copy-start.8 = (f32[2048]{0:T(1024)S(1)}, f32[2048]{0:T(1024)}, u32[]{:S(2)}) copy-start(f32[2048]{0:T(1024)} %param.12) | copy-start | bytes 24580
  178.7 92.9 %copy-start.6 = (f32[64,1408]{1,0:T(8,128)S(1)}, f32[64,1408]{1,0:T(8,128)}, u32[]{:S(2)}) copy-start(f32[64,1408]{1,0:T(8,128)} %param.13) | copy-start | bytes 1081348
  178.7 92.9 %copy-start.7 = (f32[64,1408]{1,0:T(8,128)S(1)}, f32[64,1408]{1,0:T(8,128)}, u32[]{:S(2)}) copy-start(f32[64,1408]{1,0:T(8,128)} %param.14) | copy-start | bytes 1081348
  178.7 88.6 %reduce-scatter.7.cloned.1.call-start = ((), (), s32[]{:S(2)}) async-start(), calls=%async_computation.9 | async-start | bytes 2228224 | tf_op jit(solution)/shard_map/reduce_scatter | solution.py:20
  191.3 194.7 %all-gather.2.cloned.1.call-start = ((), (), s32[]{:S(2)}) async-start(), calls=%async_computation.10 | async-start | bytes 4325376 | tf_op jit(solution)/shard_map/all_gather | solution.py:89
  290.4 75.3 %all-to-all-start.2 = ((bf16[64,32,176]{2,0,1:T(8,128)(2,1)}), bf16[64,32,176]{2,0,1:T(8,128)(2,1)S(1)}, u32[]{:S(2)}, u32[]{:S(2)}) async-start(bf16[64,32,176]{2,0,1:T(8,128)(2,1)} %copy.24), calls=%async_computation.4 | async-start | bytes 2097152 | tf_op jit(solution)/shard_map/all_to_all | solution.py:54
  314.4 57.1 %copy-start.5 = (f32[176,512]{1,0:T(8,128)S(1)}, f32[176,512]{1,0:T(8,128)}, u32[]{:S(2)}) copy-start(f32[176,512]{1,0:T(8,128)} %param.15) | copy-start | bytes 1081348
  365.7 61.5 %all-to-all-start.3 = ((bf16[64,32,176]{2,0,1:T(8,128)(2,1)}), bf16[64,32,176]{2,0,1:T(8,128)(2,1)}, u32[]{:S(2)}, u32[]{:S(2)}) async-start(bf16[64,32,176]{2,0,1:T(8,128)(2,1)} %copy.25), calls=%async_computation.5 | async-start | bytes 2097152 | tf_op jit(solution)/shard_map/all_to_all | solution.py:55
  371.4 80.1 %reduce-scatter.9.cloned.1.call-start = ((), (), s32[]{:S(2)}) async-start(), calls=%async_computation.11 | async-start | bytes 6291456 | tf_op jit(solution)/shard_map/reduce_scatter | solution.py:20
  439.7 87.9 %reduce-scatter.11.cloned.1.call-start = ((), (), s32[]{:S(2)}) async-start(), calls=%async_computation.12 | async-start | bytes 2228224 | tf_op jit(solution)/shard_map/reduce_scatter | solution.py:20
  452.9 78.9 %copy-start.1 = (bf16[176,2048]{1,0:T(8,128)(2,1)S(1)}, bf16[176,2048]{1,0:T(8,128)(2,1)}, u32[]{:S(2)}) copy-start(bf16[176,2048]{1,0:T(8,128)(2,1)} %copy-done) | copy-start | bytes 2162692
  452.9 79.8 %copy-start.2 = (bf16[176,2048]{1,0:T(8,128)(2,1)S(1)}, bf16[176,2048]{1,0:T(8,128)(2,1)}, u32[]{:S(2)}) copy-start(bf16[176,2048]{1,0:T(8,128)(2,1)} %all_gather.27) | copy-start | bytes 2162692
Sparse Core Ops, SparseCore 0:
  178.9 12.3 reduce-scatter.4
  193.8 73.4 reduce-scatter.6
  271.6 98.2 all-gather.1
  439.8 11.7 reduce-scatter.8
  454.0 73.5 reduce-scatter.10
where the time goes:
time: 541 us; the launch traced here: 540 us
  waiting for transfers between devices  326 us (60%)
  blocking collectives  101 us (19%)
  local copies, waits for them, and re-layouts  35.6 us (7%)
  starting transfers between devices  30.2 us (6%)
  matrix products  23.2 us (4%)
  between operations  14 us (3%)
  other arithmetic  9.45 us (2%)
    reduce_scatter x4, waiting for transfers between devices, reduced_to_own(): pieces = lax.psum_scatter(pieces, axes[k], scatter_dimension=0, tiled=True)  170 us
    all_to_all x2, waiting for transfers between devices, relay_weights(): lax.all_to_all(gate_rows, FS, split_axis=1, concat_axis=0, tiled=True)  82 us
    all_to_all x2, waiting for transfers between devices, relay_weights(): lax.all_to_all(up_rows, FS, split_axis=1, concat_axis=0, tiled=True)  73.9 us
    all_gather x2, blocking collectives, relay_weights(): lax.all_gather(gate_proj, 'tp', axis=1, tiled=True)  43.7 us
    all_gather x2, blocking collectives, relay_weights(): lax.all_gather(down_proj, 'tp', axis=1, tiled=True)  28.7 us
    all_gather x2, blocking collectives, relay_weights(): lax.all_gather(up_proj, 'tp', axis=1, tiled=True)  28.6 us
    all_to_all x2, starting transfers between devices, relay_weights(): lax.all_to_all(gate_rows, FS, split_axis=1, concat_axis=0, tiled=True)  19.4 us
    dot_general x2, matrix products, row_terms(): return jnp.dot(hidden, down_proj, preferred_element_type=jnp.float32)  14.6 us
  transfers between devices with their start and end apart: 9, of which 8 were waited for; matrix products, arithmetic and copies ran while one was open for 4% of the time, Pallas kernels for 0%

commit v1 on v0

v1 whole, which is shorter than its diff:
```python
import functools

import jax
import jax.numpy as jnp
from jax import lax
from jax.experimental import pallas as pl
from jax.experimental.pallas import tpu as pltpu
from jax.sharding import PartitionSpec as P

norm_eps = 1e-05
deep_alpha = 2.0**0.25
half_step = 0.5

LANES = 128
SUBS = 4
TILE_Z = 4
MESH = pl.DeviceIdType.MESH


def plain_norm(values):
    row_mean = jnp.mean(values, axis=-1, keepdims=True)
    centred = values - row_mean
    variance = jnp.mean(centred * centred, axis=-1, keepdims=True)
    return centred * lax.rsqrt(variance + norm_eps)


def split_widths(width):
    main = width // LANES * LANES
    tail = width - main
    return main, tail, -(-2 * tail // LANES) * LANES


def pack_pair(gate, up, tp_size, served):
    rows = gate.shape[0]
    gate = gate.reshape(rows, served, -1)
    up = up.reshape(rows, served, -1)
    main, tail, tail_room = split_widths(gate.shape[-1])
    pieces = [gate[..., :main], up[..., :main], gate[..., main:], up[..., main:]]
    pieces.append(jnp.zeros((rows, served, tail_room - 2 * tail), gate.dtype))
    packed = jnp.concatenate(pieces, axis=-1)
    packed = packed.reshape(tp_size, rows // tp_size, served, packed.shape[-1])
    return packed.transpose(0, 2, 1, 3)


def unpack_pair(packed, width):
    main, tail, _ = split_widths(width)
    packed = packed.reshape(-1, packed.shape[-1])
    gate = jnp.concatenate([packed[:, :main], packed[:, 2 * main : 2 * main + tail]], axis=-1)
    up = jnp.concatenate(
        [packed[:, main : 2 * main], packed[:, 2 * main + tail : 2 * main + 2 * tail]], axis=-1
    )
    return gate, up


def kernel(
    n_fs,
    n_tp,
    width,
    x_in,
    gain,
    src1,
    src2,
    dsrc1,
    dsrc2,
    res_out,
    gu1_out,
    gu2_out,
    dn1_out,
    dn2_out,
    x1,
    x2,
    st1,
    st2,
    gu1,
    gu2,
    dn1,
    dn2,
    part1,
    part2,
    xch1,
    xch2,
    ring1,
    ring2,
    loc_sem,
    out_sem,
    p1_recv,
    p2_recv,
    p3_recv,
    dn_recv,
    xch_recv,
    rs_recv,
    ag_recv,
    sib_recv,
    send_sem,
):
    n_z = n_fs // 2
    half = n_z // 2
    served = n_fs // n_tp
    main, tail, tail_room = split_widths(width)
    me = lax.axis_index("fs")
    me_x = lax.axis_index("tp")
    z, c = me // 2, lax.rem(me, 2)
    sib = me + 1 - 2 * c
    x_right, x_left = lax.rem(me_x + 1, n_tp), lax.rem(me_x + n_tp - 1, n_tp)
    z_right = 2 * lax.rem(z + 1, n_z) + c
    z_left = 2 * lax.rem(z + n_z - 1, n_z) + c
    own, features = x1.shape[2], x1.shape[3]
    sub = features // SUBS
    dcols = dsrc1.shape[1]
    d_cut = width // 32 * 16 + 16

    def remote(src, dst, send, recv, **device):
        return pltpu.make_async_remote_copy(
            src_ref=src, dst_ref=dst, send_sem=send, recv_sem=recv, device_id=device, device_id_type=MESH
        )

    def wait_for(ref, sem):
        pltpu.make_async_copy(ref, ref, sem).wait()

    def d_at(ref, col_block, first=0, size=width):
        return ref.at[pl.ds(first, size), pl.ds(pl.multiple_of(col_block * dcols, dcols), dcols)]

    local = [
        pltpu.make_async_copy(src1.at[me_x], st1.at[me_x], loc_sem.at[0]),
        pltpu.make_async_copy(src2.at[me_x], st2.at[me_x], loc_sem.at[1]),
        pltpu.make_async_copy(dsrc1, d_at(dn1, me_x), loc_sem.at[2]),
        pltpu.make_async_copy(dsrc2, d_at(dn2, me_x), loc_sem.at[3]),
        pltpu.make_async_copy(x_in, x1, loc_sem.at[4]),
    ]
    for copy in local:
        copy.start()

    barrier = pltpu.get_barrier_semaphore()

    def greet_fs(i, carry):
        pl.semaphore_signal(barrier, inc=1, device_id={"fs": lax.rem(me + i, n_fs)}, device_id_type=MESH)
        return carry

    def greet_tp(i, carry):
        pl.semaphore_signal(barrier, inc=1, device_id={"tp": lax.rem(me_x + i, n_tp)}, device_id_type=MESH)
        return carry

    lax.fori_loop(1, n_tp, greet_tp, 0)
    lax.fori_loop(1, n_fs, greet_fs, 0)
    pl.semaphore_wait(barrier, n_fs - 1 + n_tp - 1)

    def scatter_tp(b, src, st):
        for i in range(1, n_tp):
            to = lax.rem(me_x + i, n_tp)
            remote(src.at[to], st.at[me_x], send_sem.at[b, 0], p1_recv.at[b, n_tp - i - 1], tp=to).start()

    def wait_scatter(b, st):
        for i in range(1, n_tp):
            frm = lax.rem(me_x + i, n_tp)
            wait_for(st.at[frm], p1_recv.at[b, i - 1])

    def down_own(b, dsrc, dn):
        remote(dsrc, d_at(dn, me_x), send_sem.at[b, 1], dn_recv.at[b, 0], tp=x_right).start()
        remote(dsrc, d_at(dn, me_x), send_sem.at[b, 2], dn_recv.at[b, 1], tp=x_left).start()

    def down_forward(b, dn):
        wait_for(d_at(dn, x_left), dn_recv.at[b, 0])
        upper = d_at(dn, x_left, 0, d_cut)
        remote(upper, upper, send_sem.at[b, 3], dn_recv.at[b, 2], tp=x_right).start()
        wait_for(d_at(dn, x_right), dn_recv.at[b, 1])
        lower = d_at(dn, x_right, d_cut, width - d_cut)
        remote(lower, lower, send_sem.at[b, 4], dn_recv.at[b, 3], tp=x_left).start()

    def down_wait(b, dn):
        across = lax.rem(me_x + 2, n_tp)
        wait_for(d_at(dn, across, 0, d_cut), dn_recv.at[b, 2])
        wait_for(d_at(dn, across, d_cut, width - d_cut), dn_recv.at[b, 3])

    def at_distance(i):
        reach = (i + 1) // 2
        return lax.rem(z + n_z + reach * (2 * lax.rem(i, 2) - 1), n_z)

    def spread_fs(b, st, gu):
        gu[z, c, me_x] = st[me // served, lax.rem(me, served)]
        remote(
            st.at[sib // served, lax.rem(sib, served)], gu.at[z, c, me_x], send_sem.at[b, 5], p2_recv.at[b, z], fs=sib
        ).start()

        def to_chip(i, carry):
            zi = at_distance(i)
            for other in range(2):
                to = 2 * zi + other
                remote(
                    st.at[to // served, lax.rem(to, served)],
                    gu.at[z, c, me_x],
                    send_sem.at[b, 5],
                    p2_recv.at[b, z],
                    fs=to,
                ).start()
            return carry

        lax.fori_loop(1, n_z, to_chip, 0)

    def gather_own(b, gu, i):
        zi = at_distance(i)
        piece = gu.at[zi, :, me_x]
        remote(piece, piece, send_sem.at[b, 6], p3_recv.at[b, 0, i], tp=x_right).start()
        remote(piece, piece, send_sem.at[b, 7], p3_recv.at[b, 1, i], tp=x_left).start()

    def gather_own_first(b, gu):
        wait_for(gu.at[z, 1 - c, me_x], p2_recv.at[b, z])
        gather_own(b, gu, 0)

    def gather_own_next(b, gu, i):
        zi = at_distance(i)
        wait_for(gu.at[zi, :, me_x], p2_recv.at[b, zi])
        gather_own(b, gu, i)

    def gather_forward(b, gu, i):
        zi = at_distance(i)
        from_left, from_right = gu.at[zi, :, x_left], gu.at[zi, :, x_right]
        wait_for(from_left, p3_recv.at[b, 0, i])
        wait_for(from_right, p3_recv.at[b, 1, i])

        @pl.when(lax.rem(i, 2) == 0)
        def _():
            remote(from_left, from_left, send_sem.at[b, 8], p3_recv.at[b, 2, i], tp=x_right).start()

        @pl.when(lax.rem(i, 2) == 1)
        def _():
            remote(from_right, from_right, send_sem.at[b, 8], p3_recv.at[b, 2, i], tp=x_left).start()

    def gather_wait(b, gu):
        across = lax.rem(me_x + 2, n_tp)

        def one(i, carry):
            wait_for(gu.at[at_distance(i), :, across], p3_recv.at[b, 2, i])
            return carry

        lax.fori_loop(0, n_z, one, 0)

    lag = 2

    def gather_tp(b, gu):
        gather_own_first(b, gu)

        def one(i, carry):
            gather_own_next(b, gu, i)

            @pl.when(i >= lag)
            def _():
                gather_forward(b, gu, i - lag)

            return carry

        lax.fori_loop(1, n_z, one, 0)
        for i in range(n_z - lag, n_z):
            gather_forward(b, gu, jnp.int32(i))

    def compute(b, x, gu, dn, part, xch):
        n_tiles = n_z // TILE_Z
        rows = TILE_Z * 2 * own
        weights = gu[...].reshape(features, gu.shape[-1])

        def tile(i, carry):
            t = lax.rem(z // TILE_Z + n_tiles // 2 + i, n_tiles)
            tokens = x[pl.ds(t * TILE_Z, TILE_Z)].reshape(rows, features)
            act = jnp.dot(tokens, weights, preferred_element_type=jnp.float32)
            gate_main, up_main = act[:, :main], act[:, main : 2 * main]
            rest = act[:, 2 * main :]
            up_rest = pltpu.roll(rest, tail_room - tail, 1)
            lane = lax.broadcasted_iota(jnp.int32, rest.shape, 1)
            rest = jnp.where(lane < tail, jax.nn.silu(rest) * up_rest, 0.0)
            hidden = jnp.concatenate([jax.nn.silu(gate_main) * up_main, rest], axis=1).astype(jnp.bfloat16)
            for k in range(SUBS):
                cols = slice(k * sub, (k + 1) * sub)
                out = jnp.dot(hidden, dn[:, cols], preferred_element_type=jnp.float32)
                part[pl.ds(t * TILE_Z, TILE_Z), :, :, cols] = out.astype(jnp.bfloat16).reshape(
                    TILE_Z, 2, own, sub
                )

            def swap(j, carry):
                zj = t * TILE_Z + j
                remote(part.at[zj, 1 - c], xch.at[zj], send_sem.at[b, 9], xch_recv.at[b, zj], fs=sib).start()
                return carry

            lax.fori_loop(0, TILE_Z, swap, 0)
            return carry

        lax.fori_loop(0, n_tiles, tile, 0)

    def sub_of(ref, k):
        return ref.at[:, pl.ds(k * sub, sub)]

    def reduce_step(b, part, xch, ring, s, both):
        o_right = lax.rem(z + half - s + n_z, n_z)
        o_left = lax.rem(z - (half - 1) + s + 2 * n_z, n_z)
        ways = [(0, o_right, z_right, 0), (1, o_left, z_left, half)][: 2 if both else 1]
        for way, o, to, base in ways:
            wait_for(xch.at[o], xch_recv.at[b, o])
        for k in range(SUBS):
            cols = slice(k * sub, (k + 1) * sub)
            for way, o, to, base in ways:
                total = part[o, c, :, cols].astype(jnp.float32) + xch[o, :, cols].astype(jnp.float32)
                if not isinstance(s, int):
                    wait_for(sub_of(ring.at[base + s - 1], k), rs_recv.at[b, way, s - 1, k])
                    total = total + ring[base + s - 1, :, cols].astype(jnp.float32)
                part[o, c, :, cols] = total.astype(jnp.bfloat16)
                remote(
                    sub_of(part.at[o, c], k),
                    sub_of(ring.at[base + s], k),
                    send_sem.at[b, 10],
                    rs_recv.at[b, way, s, k],
                    fs=to,
                ).start()

    def reduce_rest(b, part, xch, ring):
        def one(s, carry):
            reduce_step(b, part, xch, ring, s, True)
            return carry

        lax.fori_loop(1, half - 1, one, 0)
        reduce_step(b, part, xch, ring, jnp.int32(half - 1), False)

    def reduced_own(b, part, xch, ring):
        wait_for(xch.at[z], xch_recv.at[b, z])
        for k in range(SUBS):
            wait_for(sub_of(ring.at[half - 1], k), rs_recv.at[b, 0, half - 1, k])
            wait_for(sub_of(ring.at[2 * half - 2], k), rs_recv.at[b, 1, half - 2, k])
        pieces = [part[z, c], xch[z], ring[half - 1], ring[2 * half - 2]]
        return sum(p.astype(jnp.float32) for p in pieces)

    def to_sibling(zi):
        chunk = x2.at[zi, c]
        remote(chunk, chunk, send_sem.at[1, 11], sib_recv.at[zi], fs=sib).start()

    def share_step(s, first, left):
        z_from_left = lax.rem(z - s + 2 * n_z, n_z)
        z_from_right = lax.rem(z + s, n_z)
        for k in range(SUBS):
            for way, zi, to, send in [(0, z_from_left, z_right, True), (1, z_from_right, z_left, left)]:
                chunk = sub_of(x2.at[zi, c], k)
                if not first:
                    wait_for(chunk, ag_recv.at[way, s - 1, k])
                if send:
                    remote(chunk, chunk, send_sem.at[0, 11], ag_recv.at[way, s, k], fs=to).start()
        if first:
            to_sibling(z)
        else:
            to_sibling(z_from_left)
            to_sibling(z_from_right)

    def share_tokens():
        share_step(0, True, True)

        def one(s, carry):
            share_step(s, False, True)
            return carry

        lax.fori_loop(1, half - 1, one, 0)
        share_step(jnp.int32(half - 1), False, False)
        far = lax.rem(z + half, n_z)
        for k in range(SUBS):
            wait_for(sub_of(x2.at[far, c], k), ag_recv.at[0, half - 1, k])
        to_sibling(far)

        def sibling_done(zi, carry):
            wait_for(x2.at[zi, 1 - c], sib_recv.at[zi])
            return carry

        lax.fori_loop(0, n_z, sibling_done, 0)

    for copy in local[2:4]:
        copy.wait()
    for dn in (dn1, dn2):
        dn[width:, :] = jnp.zeros((dn.shape[0] - width, features), jnp.bfloat16)

    scatter_tp(0, src1, st1)
    scatter_tp(1, src2, st2)
    down_own(0, dsrc1, dn1)
    local[0].wait()
    wait_scatter(0, st1)
    spread_fs(0, st1, gu1)
    local[1].wait()
    wait_scatter(1, st2)
    spread_fs(1, st2, gu2)
    down_forward(0, dn1)
    gather_tp(0, gu1)
    gather_wait(0, gu1)
    down_wait(0, dn1)
    outs = [
        pltpu.make_async_copy(gu1, gu1_out, out_sem.at[0]),
        pltpu.make_async_copy(dn1.at[pl.ds(0, width)], dn1_out, out_sem.at[1]),
    ]
    for copy in outs:
        copy.start()
    down_own(1, dsrc2, dn2)
    local[4].wait()
    compute(0, x1, gu1, dn1, part1, xch1)
    reduce_step(0, part1, xch1, ring1, 0, True)
    gather_tp(1, gu2)
    down_forward(1, dn2)
    reduce_rest(0, part1, xch1, ring1)
    ffn_one = reduced_own(0, part1, xch1, ring1)
    normed = plain_norm(deep_alpha * x1[z, c].astype(jnp.float32) + half_step * ffn_one)
    x2[z, c] = normed.astype(jnp.bfloat16)
    share_tokens()
    gather_wait(1, gu2)
    down_wait(1, dn2)
    more = [
        pltpu.make_async_copy(gu2, gu2_out, out_sem.at[2]),
        pltpu.make_async_copy(dn2.at[pl.ds(0, width)], dn2_out, out_sem.at[3]),
    ]
    for copy in more:
        copy.start()
    compute(1, x2, gu2, dn2, part2, xch2)
    reduce_step(1, part2, xch2, ring2, 0, True)
    reduce_rest(1, part2, xch2, ring2)
    ffn_two = reduced_own(1, part2, xch2, ring2)
    residual = deep_alpha * gain[...] * x2[z, c].astype(jnp.float32)
    res_out[...] = plain_norm(residual + half_step * ffn_two).astype(jnp.bfloat16)

    for copy in outs + more:
        copy.wait()
    for b, src, st, gu, dsrc, dn, xch, ring in (
        (0, src1, st1, gu1, dsrc1, dn1, xch1, ring1),
        (1, src2, st2, gu2, dsrc2, dn2, xch2, ring2),
    ):
        wait_for(st.at[pl.ds(0, n_tp - 1)], send_sem.at[b, 0])
        wait_for(d_at(dn, me_x), send_sem.at[b, 1])
        wait_for(d_at(dn, me_x), send_sem.at[b, 2])
        wait_for(d_at(dn, x_left, 0, d_cut), send_sem.at[b, 3])
        wait_for(d_at(dn, x_right, d_cut, width - d_cut), send_sem.at[b, 4])
        flat = st.reshape(n_fs, *st.shape[2:])
        wait_for(flat.at[pl.ds(0, n_fs - 1)], send_sem.at[b, 5])
        wait_for(gu.at[:, :, me_x], send_sem.at[b, 6])
        wait_for(gu.at[:, :, me_x], send_sem.at[b, 7])
        wait_for(gu.at[:, :, me_x], send_sem.at[b, 8])
        wait_for(xch, send_sem.at[b, 9])
        wait_for(ring, send_sem.at[b, 10])
    wait_for(ring1, send_sem.at[0, 11])
    wait_for(xch1, send_sem.at[1, 11])


def body(prompt, gate_first, up_first, down_first, norm_gain, gate_second, up_second, down_second):
    n_fs, n_tp = lax.axis_size("fs"), lax.axis_size("tp")
    n_z, served = n_fs // 2, n_fs // n_tp
    half = n_z // 2
    features = prompt.shape[-1]
    own = prompt.shape[-2] // n_fs
    width = down_first.shape[0]
    wide = -(-width // LANES) * LANES
    bf16 = jnp.bfloat16
    row_block = gate_first.shape[0]
    gain_rows = lax.dynamic_slice_in_dim(norm_gain, lax.axis_index("fs") * row_block, row_block, 0)[:, None]

    src1 = pack_pair(gate_first.astype(bf16), up_first.astype(bf16), n_tp, served)
    src2 = pack_pair(
        (gain_rows * gate_second).astype(bf16), (gain_rows * up_second).astype(bf16), n_tp, served
    )
    tokens = prompt.reshape(n_z, 2, own, features)
    gu_shape = (n_z, 2, n_tp, row_block // n_tp, src1.shape[-1])
    hbm = pl.BlockSpec(memory_space=pltpu.HBM)
    vmem = pl.BlockSpec(memory_space=pltpu.VMEM)
    dma = pltpu.SemaphoreType.DMA
    result, gu1, gu2, down_one, down_two = pl.pallas_call(
        functools.partial(kernel, n_fs, n_tp, width),
        out_shape=[
            jax.ShapeDtypeStruct((own, features), bf16),
            jax.ShapeDtypeStruct(gu_shape, bf16),
            jax.ShapeDtypeStruct(gu_shape, bf16),
            jax.ShapeDtypeStruct((width, features), bf16),
            jax.ShapeDtypeStruct((width, features), bf16),
        ],
        in_specs=[hbm, vmem, hbm, hbm, hbm, hbm],
        out_specs=[vmem, hbm, hbm, hbm, hbm],
        scratch_shapes=[
            pltpu.VMEM((n_z, 2, own, features), bf16),
            pltpu.VMEM((n_z, 2, own, features), bf16),
            pltpu.VMEM(src1.shape, bf16),
            pltpu.VMEM(src1.shape, bf16),
            pltpu.VMEM(gu_shape, bf16),
            pltpu.VMEM(gu_shape, bf16),
            pltpu.VMEM((wide, features), bf16),
            pltpu.VMEM((wide, features), bf16),
            pltpu.VMEM((n_z, 2, own, features), bf16),
            pltpu.VMEM((n_z, 2, own, features), bf16),
            pltpu.VMEM((n_z, own, features), bf16),
            pltpu.VMEM((n_z, own, features), bf16),
            pltpu.VMEM((n_z - 1, own, features), bf16),
            pltpu.VMEM((n_z - 1, own, features), bf16),
            dma((5,)),
            dma((4,)),
            dma((2, n_tp - 1)),
            dma((2, n_z)),
            dma((2, 3, n_z)),
            dma((2, 4)),
            dma((2, n_z)),
            dma((2, 2, half, SUBS)),
            dma((2, half, SUBS)),
            dma((n_z,)),
            dma((2, 12)),
        ],
        compiler_params=pltpu.CompilerParams(
            collective_id=0, has_side_effects=True, vmem_limit_bytes=60 * 1024 * 1024
        ),
    )(tokens, norm_gain[None, :], src1, src2, down_first.astype(bf16), down_second.astype(bf16))
    gate_one, up_one = unpack_pair(gu1, width)
    gate_two, up_two = unpack_pair(gu2, width)
    return (result[None], gate_one, up_one, down_one, gate_two, up_two, down_two)


def solution(mesh):
    weight = P("fs", "tp")
    return jax.shard_map(
        body,
        mesh=mesh,
        in_specs=(P(("grp", "tp"), None, None), weight, weight, weight, P(), weight, weight, weight),
        out_specs=(
            P(("grp", "tp"), "fs", None),
            P("grp", "fs"),
            P("grp", "fs"),
            P("fs", "grp"),
            P("grp", "fs"),
            P("grp", "fs"),
            P("fs", "grp"),
        ),
        check_vma=False,
    )
```

time: 541 us -> 206 us (0.38)
  waiting for transfers between devices: 326 us -> 0 us
  Pallas kernels: 0 us -> 189 us
  blocking collectives: 101 us -> 0 us
  starting transfers between devices: 30.2 us -> 0 us
  local copies, waits for them, and re-layouts: 35.6 us -> 10.1 us
  matrix products: 23.2 us -> 0 us
  between operations: 14 us -> 0.92 us
    pallas_call x0 -> x1, Pallas kernels: none -> 189 us  [body(): pl.pallas_call(functools.partial(kernel, n_fs, n_tp, width), out_shape=[j...]
    reduce_scatter x4 -> x0, waiting for transfers between devices: 170 us -> none  [reduced_to_own(): pieces = lax.psum_scatter(pieces, axes[k], scatter_dimension=0, tiled=True)]
    all_to_all x4 -> x0, waiting for transfers between devices: 156 us -> none  [the longest x2 82 us: relay_weights(): lax.all_to_all(gate_rows, FS, split_axis=1, concat_axis=0, tiled=True)]
    all_gather x6 -> x0, blocking collectives: 101 us -> none  [the longest x2 43.7 us: relay_weights(): lax.all_gather(gate_proj, 'tp', axis=1, tiled=True)]
    all_to_all x4 -> x0, starting transfers between devices: 29.9 us -> none  [the longest x2 19.4 us: relay_weights(): lax.all_to_all(gate_rows, FS, split_axis=1, concat_axis=0, tiled=True)]
    dot_general x4 -> x0, matrix products: 23.2 us -> none  [the longest x2 14.6 us: row_terms(): return jnp.dot(hidden, down_proj, preferred_element_type=jnp.float32)]
    all_to_all x8 -> x0, local copies, waits for them, and re-layouts: 18.4 us -> none  [the longest x4 10.2 us: relay_weights(): lax.all_to_all(up_rows, FS, split_axis=1, concat_axis=0, tiled=True)]
    transpose x2 -> x1, local copies, waits for them, and re-layouts: 9.44 us -> 0.99 us  [pack_pair(): return packed.transpose(0, 2, 1, 3)]
  transfers between devices with their start and end apart: 9 -> 0, of which waited for: 8 -> 0; matrix products, arithmetic and copies ran while one was open for 4% -> 0% of each run, Pallas kernels for 0% -> 0%
where the time goes in v1:
time: 206 us
  Pallas kernels  189 us (92%)
  local copies, waits for them, and re-layouts  10.1 us (5%)
  other arithmetic  6.26 us (3%)
    pallas_call x1, Pallas kernels, body(): pl.pallas_call(functools.partial(kernel, n_fs, n_tp, width), out_shape=[j...  189 us
    unnamed x29, local copies, waits for them, and re-layouts  4.36 us

profile of v1, /device:TPU:34, one launch (start us, length us, event | category | flops | bytes accessed | tf_op | source)
XLA Modules:
  0.0 205.9 jit_solution(11196727265531714800)
XLA Ops:
  0.6 0.8 dynamic_slice.3
  1.4 1.2 multiply_convert_fusion
  2.6 0.4 reshape.46
  3.0 0.4 reshape.47
  3.5 0.2 concatenate.19
  3.8 0.2 copy-done.4
  4.0 0.4 reshape.43
  4.5 0.4 reshape.44
  4.9 0.2 concatenate.18
  5.2 1.0 copy_bitcast_fusion
  6.2 0.7 convert_element_type.22.dsrc1
  6.9 0.7 convert_element_type.23.dsrc2
  7.6 188.6 %shard_map.135 = (bf16[32,2048]{1,0:T(8,128)(2,1)}, bf16[16,2,4,16,384]{4,3,2,1,0:T(8,128)(2,1)}, bf16[16,2,4,16,384]{4,3,2,1,0:T(8,128)(2,1)}, bf16[176,2048]{1,0:T(8,128)(2,1)}, bf16[176,2048]{1,0:T(8,128)(2,1)}) custom-call(bf16[16,2,32,2048]{3,2,1,0:T(8,128)(2,1)} %bitcast.11, f32[1,2048]{1,0:T(1,128)} %bitcast.19, ...), custom_call_target="tpu_custom_call" | custom-call | tf_op jit(solution)/shard_map/pallas_call | solution.py:461
  196.2 1.5 fusion.3
  197.7 0.2 copy.34
  197.9 0.1 fusion.2
  198.0 0.2 copy.33
  198.2 0.9 pad_maximum_fusion
  199.1 0.2 copy.36
  199.3 0.2 copy.35
  199.5 0.9 pad_maximum_fusion.1
  200.4 0.1 copy-done
  200.5 0.2 fusion.1
  200.8 0.2 copy.38
  201.0 0.2 copy.37
  201.3 0.9 pad_maximum_fusion.2
  202.2 0.2 copy.40
  202.4 0.2 copy.39
  202.6 0.9 pad_maximum_fusion.3
  203.5 0.7 copy.46
  204.2 0.9 copy.47
  205.0 0.9 copy.48
  (28 shorter events, 0.3 us)
Async XLA Ops:
  3.0 1.0 copy-start.4
  3.4 1.0 copy-start.5
  4.9 1.3 copy-start.6
  4.9 1.9 copy-start.7
  196.1 1.7 copy-start.1
  199.1 1.4 copy-start
  202.2 1.3 copy-start.8
  202.4 1.8 copy-start.3
  202.6 2.4 %copy-start.2 = (bf16[176,2048]{1,0:T(8,128)(2,1)S(1)}, bf16[176,2048]{1,0:T(8,128)(2,1)}, u32[]{:S(2)}) copy-start(bf16[176,2048]{1,0:T(8,128)(2,1)} %get-tuple-element.42) | copy-start | bytes 2162692
